TPU v7x, 32 devices: a whole 2x2x4 slice. The times are simulated.
32 devices in a mesh: grp: 2 (over y), sp: 4 (over z), tp: 4 (over x, core).
Axes of the slice: x: 2, y: 2, z: 4, core: 2. Of those that a mesh axis runs over, the one named last changes fastest.
Arguments:
- stream: bfloat16 [1024, 2048], P(('grp', 'sp')), parts along dimension 0, may hold values from -40 to 40
- queries: bfloat16 [1024, 1024], P(('grp', 'sp'), 'tp'), parts along dimension 0, may hold values from -6 to 6
- key_matrix: bfloat16 [1024, 1024], P(('grp', 'sp'), 'tp'), parts along dimension 0, may hold values from -6 to 6
- value_matrix: bfloat16 [1024, 2048], P(('grp', 'sp'), 'tp'), parts along dimension 0, may hold values from -6 to 6
- output_gate_logits: bfloat16 [1024, 2048], P(('grp', 'sp'), 'tp'), parts along dimension 0, may hold values from -6 to 6
- forgetting_raw_score: float32 [1024, 1024], P(('grp', 'sp'), 'tp'), parts along dimension 0, may hold values from -2 to 12
- additional_forgetting_rate: float32 [1024, 1024], P(('grp', 'sp'), 'tp'), parts along dimension 0, may hold values from -0.7 to 0
- head_norm_gain: float32 [2048], P('tp'), may hold values from 0.1 to 1.9
- output_weight: bfloat16 [2048, 2048], P('tp'), may hold values from -0.125 to 0.125
- feedforward_norm_gain: bfloat16 [2048], replicated, may hold values from 0.099609375 to 1.8984375
- gate_weight: bfloat16 [2048, 5632], P('sp', 'tp'), may hold values from -0.125 to 0.125
- up_weight: bfloat16 [2048, 5632], P('sp', 'tp'), may hold values from -0.125 to 0.125
- down_weight: bfloat16 [5632, 2048], P('tp', 'sp'), may hold values from -0.078125 to 0.078125
Outputs:
- layer_out: bfloat16 [1024, 2048], P(('grp', 'sp'), 'tp'), parts along dimension 0
There are 2 independent parts, one for each index of `grp`. A program takes and returns all parts, laid end to end along the dimension named above; an argument that names none is the same for every part. Nothing has to cross between parts.
All inputs are finite; a program needn't handle non-finite values.
Results may differ from a plain program's by a relative error of at most 0.013.
Values may be sent and summed in bfloat16 or wider, within the bound.
A program may use at most 128 MiB of HBM per device.

v0:
```python
import jax
import jax.numpy as jnp
from jax import lax
from jax.sharding import PartitionSpec as P

HK = 256
HV = 512
BLOCK = 64
epsilon = 1e-06
sigmoid_sharpness = 16.0
highest = lax.Precision.HIGHEST


def carried_in(value, axis, join, neutral):
    place = lax.axis_index(axis)
    gathered = jax.tree.map(
        lambda a, kind: lax.all_gather(a.astype(kind), axis), value, (jnp.bfloat16, jnp.bfloat16)
    )
    state = jax.tree.map(lambda a, e: jnp.zeros_like(a) + jnp.asarray(e, a.dtype), value, neutral)

    def one(turn, state):
        return join(
            state,
            jax.tree.map(
                lambda a, own: lax.dynamic_index_in_dim(a, turn, 0, False).astype(own.dtype),
                gathered,
                value,
            ),
        )

    return lax.fori_loop(0, place, one, state)


def split_heads(tensor, blocks, count, depth):
    return tensor.astype(jnp.float32).reshape(blocks, BLOCK, count, depth).transpose(2, 0, 1, 3)


def combine(earlier, later):
    return (earlier[0] * later[0], later[0][:, :, None] * earlier[1] + later[1])


def local(
    stream,
    queries,
    key_matrix,
    value_matrix,
    output_gate_logits,
    forgetting_raw_score,
    additional_forgetting_rate,
    head_norm_gain,
    output_weight,
    feedforward_norm_gain,
    gate_weight,
    up_weight,
    down_weight,
):
    tokens = queries.shape[0]
    owned_heads = queries.shape[1] // HK
    blocks = tokens // BLOCK
    forgetting_exponent = (
        jax.nn.log_sigmoid(forgetting_raw_score) / sigmoid_sharpness + additional_forgetting_rate
    )
    query_part = split_heads(queries, blocks, owned_heads, HK) * HK ** (-0.5)
    key_part = split_heads(key_matrix, blocks, owned_heads, HK)
    value_part = split_heads(value_matrix, blocks, owned_heads, HV)
    decay_part = split_heads(forgetting_exponent, blocks, owned_heads, HK)
    within = jnp.cumsum(decay_part, axis=2)
    closing = within[:, :, -1, :]
    query_in = query_part * jnp.exp(within)
    key_in = key_part * jnp.exp(-within)
    key_end = key_part * jnp.exp(closing[:, :, None, :] - within)
    causal = jnp.tril(jnp.ones((BLOCK, BLOCK), jnp.bool_))
    scores = jnp.einsum("hntd,hnsd->hnts", query_in, key_in, precision=highest)
    scores = jnp.where(causal, scores, 0.0)
    inside = jnp.einsum("hnts,hnsv->hntv", scores, value_part, precision=highest)

    def advance(memory, inputs):
        query_block, key_block, value_block, decay_block = inputs
        final_answer = jnp.einsum("htd,hdv->htv", query_block, memory, precision=highest)
        memory = decay_block[:, :, None] * memory + jnp.einsum(
            "hsd,hsv->hdv", key_block, value_block, precision=highest
        )
        return (memory, final_answer)

    sequence = (
        jnp.moveaxis(query_in, 1, 0),
        jnp.moveaxis(key_end, 1, 0),
        jnp.moveaxis(value_part, 1, 0),
        jnp.moveaxis(jnp.exp(closing), 1, 0),
    )
    start_memory = jnp.zeros((owned_heads, HK, HV), jnp.float32)
    final_memory, earlier_blocks = lax.scan(advance, start_memory, sequence)
    device_decay = jnp.exp(jnp.sum(closing, axis=1))
    neutral = (jnp.ones_like(device_decay), jnp.zeros_like(final_memory))
    _, carried = carried_in((device_decay, final_memory), "sp", combine, neutral)
    before = jnp.cumsum(closing, axis=1) - closing
    query_far = query_in * jnp.exp(before[:, :, None, :])
    outside = jnp.einsum("hntd,hdv->hntv", query_far, carried, precision=highest)
    mixed_heads = inside + jnp.moveaxis(earlier_blocks, 0, 1) + outside
    mixed_heads = mixed_heads.transpose(1, 2, 0, 3).reshape(tokens, owned_heads, HV)
    mixed_heads = mixed_heads * lax.rsqrt(
        jnp.mean(mixed_heads * mixed_heads, axis=-1, keepdims=True) + epsilon
    )
    gated_rows = (
        mixed_heads.reshape(tokens, owned_heads * HV)
        * head_norm_gain
        * jax.nn.silu(output_gate_logits.astype(jnp.float32))
    ).astype(jnp.bfloat16)
    partial_out = jnp.dot(gated_rows, output_weight, preferred_element_type=jnp.float32)
    model_width = stream.shape[1]
    column_share = model_width // lax.axis_size("tp")
    column_start = lax.axis_index("tp") * column_share
    attn_cols = lax.psum_scatter(
        partial_out.astype(jnp.bfloat16), "tp", scatter_dimension=1, tiled=True
    ).astype(jnp.float32)
    resid_part = (
        lax.dynamic_slice_in_dim(stream, column_start, column_share, 1).astype(jnp.float32)
        + attn_cols
    )
    elementwise_power = lax.psum(jnp.sum(resid_part * resid_part, axis=1), "tp")
    gain_part = lax.dynamic_slice_in_dim(
        feedforward_norm_gain, column_start, column_share, 0
    ).astype(jnp.float32)
    rescaled_portion = (
        resid_part * lax.rsqrt(elementwise_power / model_width + epsilon)[:, None] * gain_part
    ).astype(jnp.bfloat16)
    normed = lax.all_gather(rescaled_portion, "tp", axis=1, tiled=True)
    gate_sum = jnp.dot(
        normed,
        lax.all_gather(gate_weight, "sp", axis=0, tiled=True),
        preferred_element_type=jnp.float32,
    )
    up_sum = jnp.dot(
        normed,
        lax.all_gather(up_weight, "sp", axis=0, tiled=True),
        preferred_element_type=jnp.float32,
    )
    hidden = (jax.nn.silu(gate_sum) * up_sum).astype(jnp.bfloat16)
    down_sum = jnp.dot(
        hidden,
        lax.all_gather(down_weight, "sp", axis=1, tiled=True),
        preferred_element_type=jnp.float32,
    )
    ffn_part = lax.psum_scatter(
        down_sum.astype(jnp.bfloat16), "tp", scatter_dimension=1, tiled=True
    ).astype(jnp.float32)
    return (resid_part + ffn_part).astype(jnp.bfloat16)


def solution(mesh):
    return jax.shard_map(
        local,
        mesh=mesh,
        in_specs=(
            P(("grp", "sp"), None),
            P(("grp", "sp"), "tp"),
            P(("grp", "sp"), "tp"),
            P(("grp", "sp"), "tp"),
            P(("grp", "sp"), "tp"),
            P(("grp", "sp"), "tp"),
            P(("grp", "sp"), "tp"),
            P("tp"),
            P("tp", None),
            P(),
            P("sp", "tp"),
            P("sp", "tp"),
            P("tp", "sp"),
        ),
        out_specs=P(("grp", "sp"), "tp"),
        check_vma=False,
    )
```

profile of v0, /device:TPU:0, one launch (start us, length us, event | category | flops | bytes accessed | tf_op | source)
XLA Modules:
  0.0 430.0 jit_solution(5797290989619579910)
XLA Ops:
  6.5 1.2 fusion.27
  8.0 0.9 convert_element_type.88
  8.9 0.9 convert.4
  9.8 1.5 bitcast_multiply_fusion.1
  11.4 3.6 while.26
  11.4 1.1 fusion.60
  12.5 0.7 fusion.59
  13.2 1.1 fusion.60
  14.3 0.7 fusion.59
  15.0 0.7 convert_element_type.91
  15.8 12.6 %all-gather.2 = bf16[4,1,256]{2,1,0:T(2,128)(2,1)S(1)} all-gather(bf16[1,1,256]{2,1,0:T(2,128)(2,1)S(1)} %reshape.243), channel_id=2, replica_groups=mesh['grp'=2,'sp'=4,'tp'=4] {'sp'}, dimensions={0}, use_global_device_ids=true | all-gather | bytes 2560 | tf_op jit(solution)/shard_map/all_gather | solution.py:17
  28.5 0.3 convolution_select_fusion
  28.8 1.3 convolution_add_fusion.1
  30.1 16.3 %all-gather.14.cloned.1.call-done = bf16[4,256,512]{2,1,0:T(8,128)(2,1)} async-done(((bf16[1,256,512]{2,1,0:T(8,128)(2,1)}), bf16[4,256,512]{2,1,0:T(8,128)(2,1)}) %all-gather.14.cloned.1.call-update) | async-done | bytes 1048592 | tf_op jit(solution)/shard_map/all_gather | solution.py:17
  46.5 0.5 multiply_reduce_fusion.1
  47.2 1.2 convolution_convert_fusion
  48.6 0.7 all-gather.8.cloned.1.call-update
  49.3 0.5 all-gather.10.cloned.1.call-update
  49.9 0.5 all-gather.12.cloned.1.call-update
  50.5 0.8 dynamic-slice_convert_fusion.1
  51.2 22.1 %reduce-scatter.3.cloned.1.call-done = bf16[128,512]{1,0:T(8,128)(2,1)} async-done(((bf16[128,2048]{1,0:T(8,128)(2,1)}), bf16[128,512]{1,0:T(8,128)(2,1)}) %reduce-scatter.3.cloned.1.call-update) | async-done | bytes 131088 | tf_op jit(solution)/shard_map/reduce_scatter | solution.py:113
  73.3 1.1 multiply_reduce_fusion
  74.4 5.8 %psum.7 = f32[128]{0:T(128)S(1)} all-reduce(f32[128]{0:T(128)S(1)} %multiply_reduce_fusion), channel_id=1, replica_groups=mesh['grp'=2,'sp'=4,'tp'=4] {'tp'}, use_global_device_ids=true, to_apply=%region_10.11 | all-reduce | flops 128 | bytes 1024 | tf_op jit(solution)/shard_map/psum | solution.py:120
  80.2 1.1 multiply_convert_fusion
  81.2 6.9 %all_gather.25 = bf16[128,2048]{1,0:T(8,128)(2,1)S(1)} all-gather(bf16[128,512]{1,0:T(8,128)(2,1)S(1)} %multiply_convert_fusion), channel_id=1, replica_groups=mesh['grp'=2,'sp'=4,'tp'=4] {'tp'}, dimensions={1}, use_global_device_ids=true | all-gather | bytes 655360 | tf_op jit(solution)/shard_map/all_gather | solution.py:127
  88.1 93.5 %all-gather.8.cloned.1.call-done = bf16[2048,1408]{1,0:T(8,128)(2,1)} async-done(((bf16[512,1408]{1,0:T(8,128)(2,1)}), bf16[2048,1408]{1,0:T(8,128)(2,1)}) %all-gather.8.cloned.1.call-update) | async-done | bytes 5767184 | tf_op jit(solution)/shard_map/all_gather | solution.py:130
  181.6 3.6 fusion.38
  185.3 102.8 %all-gather.10.cloned.1.call-done = bf16[2048,1408]{1,0:T(8,128)(2,1)} async-done(((bf16[512,1408]{1,0:T(8,128)(2,1)}), bf16[2048,1408]{1,0:T(8,128)(2,1)}) %all-gather.10.cloned.1.call-update) | async-done | bytes 5767184 | tf_op jit(solution)/shard_map/all_gather | solution.py:135
  288.0 106.4 %all-gather.12.cloned.1.call-done = bf16[1408,2048]{1,0:T(8,128)(2,1)} async-done(((bf16[1408,512]{1,0:T(8,128)(2,1)}), bf16[1408,2048]{1,0:T(8,128)(2,1)}) %all-gather.12.cloned.1.call-update) | async-done | bytes 5767184 | tf_op jit(solution)/shard_map/all_gather | solution.py:141
  394.4 7.0 %convolution_convert_fusion.1 = bf16[128,2048]{1,0:T(8,128)(2,1)} fusion(bf16[1408,2048]{1,0:T(8,128)(2,1)} %all-gather.12.cloned.1.call-done, bf16[128,2048]{1,0:T(8,128)(2,1)S(1)} %all_gather.25, bf16[2048,1408]{1,0:T(8,128)(2,1)} %all-gather.10.cloned.1.call-done, f32[128,1408]{1,0:T(8,128)S(1)} %fusion.38), kind=kOutput, calls=%fused_computation.23 | convolution fusion | flops 1477738496 | bytes 13303808 | tf_op jit(solution)/shard_map/dot_general | solution.py:139
  401.5 20.0 %reduce-scatter.5.cloned.1.call-done = bf16[128,512]{1,0:T(8,128)(2,1)} async-done(((bf16[128,2048]{1,0:T(8,128)(2,1)}), bf16[128,512]{1,0:T(8,128)(2,1)}) %reduce-scatter.5.cloned.1.call-update) | async-done | bytes 131088 | tf_op jit(solution)/shard_map/reduce_scatter | solution.py:144
  421.5 1.7 add_convert_fusion
  (39 shorter events, 0.8 us)
Async XLA Ops:
  6.5 40.7 %copy-start = (bf16[512,2048]{1,0:T(8,128)(2,1)S(1)}, bf16[512,2048]{1,0:T(8,128)(2,1)}, u32[]{:S(2)}) copy-start(bf16[512,2048]{1,0:T(8,128)(2,1)} %param.25) | copy-start | bytes 6291460
  6.5 39.9 %all-gather.14.cloned.1.call-start = ((), (), s32[]{:S(2)}) async-start(), calls=%async_computation.7 | async-start | bytes 1310720 | tf_op jit(solution)/shard_map/all_gather | solution.py:17
  15.0 32.1 %copy-start.4 = (f32[512]{0:T(512)S(1)}, f32[512]{0:T(512)}, u32[]{:S(2)}) copy-start(f32[512]{0:T(512)} %param.24) | copy-start | bytes 6148
  15.7 57.6 %reduce-scatter.3.cloned.1.call-start = ((), (), s32[]{:S(2)}) async-start(), calls=%async_computation.2 | async-start | bytes 655360 | tf_op jit(solution)/shard_map/reduce_scatter | solution.py:113
  28.8 17.7 %copy-start.2 = (f32[128,256]{1,0:T(8,128)S(1)}, f32[128,256]{1,0:T(8,128)}, u32[]{:S(2)}) copy-start(f32[128,256]{1,0:T(8,128)} %get-tuple-element.167) | copy-start | bytes 393220
  28.8 18.3 %copy-start.3 = (bf16[128,512]{1,0:T(8,128)(2,1)S(1)}, bf16[128,512]{1,0:T(8,128)(2,1)}, u32[]{:S(2)}) copy-start(bf16[128,512]{1,0:T(8,128)(2,1)} %param.21) | copy-start | bytes 393220
  48.5 133.1 %all-gather.8.cloned.1.call-start = ((), (), s32[]{:S(2)}) async-start(), calls=%async_computation.3 | async-start | bytes 7208960 | tf_op jit(solution)/shard_map/all_gather | solution.py:130
  49.2 238.8 %all-gather.10.cloned.1.call-start = ((), (), s32[]{:S(2)}) async-start(), calls=%async_computation.4 | async-start | bytes 7208960 | tf_op jit(solution)/shard_map/all_gather | solution.py:135
  49.8 344.6 %all-gather.12.cloned.1.call-start = ((), (), s32[]{:S(2)}) async-start(), calls=%async_computation.5 | async-start | bytes 7208960 | tf_op jit(solution)/shard_map/all_gather | solution.py:141
  50.4 371.1 %reduce-scatter.5.cloned.1.call-start = ((), (), s32[]{:S(2)}) async-start(), calls=%async_computation.6 | async-start | bytes 655360 | tf_op jit(solution)/shard_map/reduce_scatter | solution.py:144
  185.3 236.3 %copy-start.1 = (bf16[128,512]{1,0:T(8,128)(2,1)S(1)}, bf16[128,512]{1,0:T(8,128)(2,1)}, u32[]{:S(2)}) copy-start(bf16[128,512]{1,0:T(8,128)(2,1)} %reduce-scatter.3.cloned.1.call-done) | copy-start | bytes 393220
Sparse Core Ops, SparseCore 0:
  15.9 30.5 all-gather.13
  48.9 24.3 reduce-scatter.2
  74.9 106.6 all-gather.7
  183.1 104.9 all-gather.9
  289.4 104.9 all-gather.11
  401.6 19.8 reduce-scatter.4
where the time goes:
time: 431 us; the launch traced here: 430 us
  waiting for transfers between devices  363 us (84%)
  blocking collectives  25.3 us (6%)
  matrix products  17.6 us (4%)
  between operations  13.7 us (3%)
  other arithmetic  10.2 us (2%)
    all_gather x1, waiting for transfers between devices, local(): lax.all_gather(down_weight, 'sp', axis=1, tiled=True)  106 us
    all_gather x1, waiting for transfers between devices, local(): lax.all_gather(up_weight, 'sp', axis=0, tiled=True)  103 us
    all_gather x1, waiting for transfers between devices, local(): lax.all_gather(gate_weight, 'sp', axis=0, tiled=True)  93.5 us
    reduce_scatter x1, waiting for transfers between devices, local(): lax.psum_scatter(partial_out.astype(jnp.bfloat16), 'tp', scatter_dimensio...  22.1 us
    reduce_scatter x1, waiting for transfers between devices, local(): lax.psum_scatter(down_sum.astype(jnp.bfloat16), 'tp', scatter_dimension=1...  20 us
    all_gather x1, waiting for transfers between devices, carried_in(): lax.all_gather(a.astype(kind), axis)  16.3 us
    all_gather x1, blocking collectives, carried_in(): lax.all_gather(a.astype(kind), axis)  12.6 us
  transfers between devices with their start and end apart: 6, of which 6 were waited for; matrix products, arithmetic and copies ran while one was open for 2% of the time, Pallas kernels for 0%

commit v1 on v0

--- a/solution.py
+++ b/solution.py
@@ -9,6 +9,24 @@
 epsilon = 1e-06
 sigmoid_sharpness = 16.0
 highest = lax.Precision.HIGHEST
+
+
+def ring_gather(value, axis, dim):
+    ways, here, lap = (lax.axis_size(axis), lax.axis_index(axis), value.shape[dim])
+    shape = [n * ways if d == dim else n for d, n in enumerate(value.shape)]
+    full = lax.dynamic_update_slice_in_dim(
+        jnp.zeros(shape, value.dtype), value, here * lap, axis=dim
+    )
+    going_up = going_down = value
+    for far in range(1, ways // 2 + 1):
+        going_up = lax.ppermute(going_up, axis, [(d, (d + 1) % ways) for d in range(ways)])
+        full = lax.dynamic_update_slice_in_dim(full, going_up, (here - far) % ways * lap, axis=dim)
+        if 2 * far < ways:
+            going_down = lax.ppermute(going_down, axis, [(d, (d - 1) % ways) for d in range(ways)])
+            full = lax.dynamic_update_slice_in_dim(
+                full, going_down, (here + far) % ways * lap, axis=dim
+            )
+    return full
 
 
 def carried_in(value, axis, join, neutral):
@@ -137,9 +155,7 @@
     )
     hidden = (jax.nn.silu(gate_sum) * up_sum).astype(jnp.bfloat16)
     down_sum = jnp.dot(
-        hidden,
-        lax.all_gather(down_weight, "sp", axis=1, tiled=True),
-        preferred_element_type=jnp.float32,
+        hidden, ring_gather(down_weight, "sp", 1), preferred_element_type=jnp.float32
     )
     ffn_part = lax.psum_scatter(
         down_sum.astype(jnp.bfloat16), "tp", scatter_dimension=1, tiled=True

time: 431 us -> 386 us (0.90)
  waiting for transfers between devices: 363 us -> 287 us
  starting transfers between devices: 0.2 us -> 17.7 us
  local copies, waits for them, and re-layouts: 0.2 us -> 14 us
    ppermute x0 -> x3, waiting for transfers between devices: none -> 130 us  [the longest x1 103 us: ring_gather(): lax.ppermute(going_down, axis, [(d, (d - 1) % ways) for d in range(ways)])]
    all_gather x1 -> x0, waiting for transfers between devices: 106 us -> none  [local(): lax.all_gather(down_weight, 'sp', axis=1, tiled=True)]
    all_gather x1, waiting for transfers between devices: 93.5 us -> 15.5 us  [local(): lax.all_gather(gate_weight, 'sp', axis=0, tiled=True)]
    reduce_scatter x1, waiting for transfers between devices: 22.1 us -> 0.01 us  [local(): lax.psum_scatter(partial_out.astype(jnp.bfloat16), 'tp', scatter_dimensio...]
    ppermute x0 -> x3, starting transfers between devices: none -> 17.6 us  [the longest x2 14.9 us: ring_gather(): lax.ppermute(going_up, axis, [(d, (d + 1) % ways) for d in range(ways)])]
    dynamic_update_slice x0 -> x4, local copies, waits for them, and re-layouts: none -> 10.6 us  [the longest x2 5.27 us: ring_gather(): lax.dynamic_update_slice_in_dim(full, going_up, (here - far) % ways * lap...]
  transfers between devices with their start and end apart: 6 -> 8, of which waited for: 6 -> 6; matrix products, arithmetic and copies ran while one was open for 2% -> 6% of each run, Pallas kernels for 0% -> 0%
where the time goes in v1:
time: 386 us; the launch traced here: 385 us
  waiting for transfers between devices  287 us (74%)
  blocking collectives  25.2 us (7%)
  starting transfers between devices  17.7 us (5%)
  matrix products  17.6 us (5%)
  local copies, waits for them, and re-layouts  14 us (4%)
  between operations  13.3 us (3%)
  other arithmetic  10.1 us (3%)
    all_gather x1, waiting for transfers between devices, local(): lax.all_gather(up_weight, 'sp', axis=0, tiled=True)  104 us
    ppermute x1, waiting for transfers between devices, ring_gather(): lax.ppermute(going_down, axis, [(d, (d - 1) % ways) for d in range(ways)])  103 us
    ppermute x2, waiting for transfers between devices, ring_gather(): lax.ppermute(going_up, axis, [(d, (d + 1) % ways) for d in range(ways)])  26.9 us
    reduce_scatter x1, waiting for transfers between devices, local(): lax.psum_scatter(down_sum.astype(jnp.bfloat16), 'tp', scatter_dimension=1...  20 us
    all_gather x1, waiting for transfers between devices, carried_in(): lax.all_gather(a.astype(kind), axis)  16.3 us
    all_gather x1, waiting for transfers between devices, local(): lax.all_gather(gate_weight, 'sp', axis=0, tiled=True)  15.5 us
    ppermute x2, starting transfers between devices, ring_gather(): lax.ppermute(going_up, axis, [(d, (d + 1) % ways) for d in range(ways)])  14.9 us
    all_gather x1, blocking collectives, carried_in(): lax.all_gather(a.astype(kind), axis)  12.7 us
  transfers between devices with their start and end apart: 8, of which 6 were waited for; matrix products, arithmetic and copies ran while one was open for 6% of the time, Pallas kernels for 0%

profile of v1, /device:TPU:0, one launch (start us, length us, event | category | flops | bytes accessed | tf_op | source)
XLA Modules:
  0.0 384.9 jit_solution(11153360449179475537)
XLA Ops:
  6.5 1.2 fusion.27
  8.0 0.9 convert_element_type.88
  8.9 0.9 convert.4
  9.8 1.5 bitcast_multiply_fusion.1
  11.4 3.6 while.26
  11.4 1.1 fusion.60
  13.2 1.1 fusion.60
  15.9 12.7 %all-gather.2 = bf16[4,1,256]{2,1,0:T(2,128)(2,1)S(1)} all-gather(bf16[1,1,256]{2,1,0:T(2,128)(2,1)S(1)} %reshape.243), channel_id=2, replica_groups=mesh['grp'=2,'sp'=4,'tp'=4] {'sp'}, dimensions={0}, use_global_device_ids=true | all-gather | bytes 2560 | tf_op jit(solution)/shard_map/all_gather | solution.py:35
  28.8 1.3 convolution_add_fusion.1
  30.2 16.3 %all-gather.11.cloned.1.call-done = bf16[4,256,512]{2,1,0:T(8,128)(2,1)} async-done(((bf16[1,256,512]{2,1,0:T(8,128)(2,1)}), bf16[4,256,512]{2,1,0:T(8,128)(2,1)}) %all-gather.11.cloned.1.call-update) | async-done | bytes 1048592 | tf_op jit(solution)/shard_map/all_gather | solution.py:35
  47.3 1.3 convolution_convert_fusion
  49.9 2.8 collective-permute-start
  52.8 2.7 collective-permute-start.1
  55.5 3.2 broadcast_in_dim.33
  58.7 2.7 constant_dynamic-update-slice_fusion.3
  61.3 26.9 %collective-permute-done = bf16[1408,512]{1,0:T(8,128)(2,1)} collective-permute-done((bf16[1408,512]{1,0:T(8,128)(2,1)}, bf16[1408,512]{1,0:T(8,128)(2,1)}, u32[]{:S(2)}, u32[]{:S(2)}) %collective-permute-start) | collective-permute-done | bytes 1441824 | tf_op jit(solution)/shard_map/ppermute | solution.py:22
  88.2 12.0 %collective-permute-start.2 = (bf16[1408,512]{1,0:T(8,128)(2,1)}, bf16[1408,512]{1,0:T(8,128)(2,1)}, u32[]{:S(2)}, u32[]{:S(2)}) collective-permute-start(bf16[1408,512]{1,0:T(8,128)(2,1)} %collective-permute-done), channel_id=1, source_target_pairs={{0,4},{4,8},{8,12},{12,0},{1,5},{5,9},{9,13},{13,1},{2,6},{6,10},{... | collective-permute-start | bytes 4325384 | tf_op jit(solution)/shard_map/ppermute | solution.py:22
  100.2 0.8 dynamic-slice_convert_fusion.1
  101.0 2.6 constant_dynamic-update-slice_fusion.2
  103.6 103.0 %collective-permute-done.1 = bf16[1408,512]{1,0:T(8,128)(2,1)} collective-permute-done((bf16[1408,512]{1,0:T(8,128)(2,1)}, bf16[1408,512]{1,0:T(8,128)(2,1)}, u32[]{:S(2)}, u32[]{:S(2)}) %collective-permute-start.1) | collective-permute-done | bytes 1441824 | tf_op jit(solution)/shard_map/ppermute | solution.py:25
  206.7 2.6 constant_dynamic-update-slice_fusion.1
  209.3 1.0 multiply_reduce_fusion
  210.3 6.1 %psum.7 = f32[128]{0:T(128)S(1)} all-reduce(f32[128]{0:T(128)S(1)} %multiply_reduce_fusion), channel_id=1, replica_groups=mesh['grp'=2,'sp'=4,'tp'=4] {'tp'}, use_global_device_ids=true, to_apply=%region_10.11 | all-reduce | flops 128 | bytes 1024 | tf_op jit(solution)/shard_map/psum | solution.py:138
  216.4 1.0 multiply_convert_fusion
  217.4 6.5 %all_gather.22 = bf16[128,2048]{1,0:T(8,128)(2,1)S(1)} all-gather(bf16[128,512]{1,0:T(8,128)(2,1)S(1)} %multiply_convert_fusion), channel_id=1, replica_groups=mesh['grp'=2,'sp'=4,'tp'=4] {'tp'}, dimensions={1}, use_global_device_ids=true | all-gather | bytes 655360 | tf_op jit(solution)/shard_map/all_gather | solution.py:145
  223.9 2.6 constant_dynamic-update-slice_fusion
  226.5 15.5 %all-gather.7.cloned.1.call-done = bf16[2048,1408]{1,0:T(8,128)(2,1)} async-done(((bf16[512,1408]{1,0:T(8,128)(2,1)}), bf16[2048,1408]{1,0:T(8,128)(2,1)}) %all-gather.7.cloned.1.call-update) | async-done | bytes 5767184 | tf_op jit(solution)/shard_map/all_gather | solution.py:148
  242.0 3.6 fusion.38
  245.7 103.9 %all-gather.9.cloned.1.call-done = bf16[2048,1408]{1,0:T(8,128)(2,1)} async-done(((bf16[512,1408]{1,0:T(8,128)(2,1)}), bf16[2048,1408]{1,0:T(8,128)(2,1)}) %all-gather.9.cloned.1.call-update) | async-done | bytes 5767184 | tf_op jit(solution)/shard_map/all_gather | solution.py:153
  349.6 7.0 %convolution_convert_fusion.1 = bf16[128,2048]{1,0:T(8,128)(2,1)} fusion(bf16[1408,2048]{1,0:T(8,128)(2,1)} %constant_dynamic-update-slice_fusion, bf16[128,2048]{1,0:T(8,128)(2,1)S(1)} %all_gather.22, bf16[2048,1408]{1,0:T(8,128)(2,1)} %all-gather.9.cloned.1.call-done, f32[128,1408]{1,0:T(8,128)S(1)} %fusion.38), kind=kOutput, calls=%fused_computation.23 | convolution fusion | flops 1477738496 | bytes 13303808 | tf_op jit(solution)/shard_map/dot_general | solution.py:157
  356.7 20.0 %reduce-scatter.5.cloned.1.call-done = bf16[128,512]{1,0:T(8,128)(2,1)} async-done(((bf16[128,2048]{1,0:T(8,128)(2,1)}), bf16[128,512]{1,0:T(8,128)(2,1)}) %reduce-scatter.5.cloned.1.call-update) | async-done | bytes 131088 | tf_op jit(solution)/shard_map/reduce_scatter | solution.py:160
  376.7 1.7 add_convert_fusion
  (49 shorter events, 4.9 us)
Async XLA Ops:
  6.5 40.7 %copy-start = (bf16[512,2048]{1,0:T(8,128)(2,1)S(1)}, bf16[512,2048]{1,0:T(8,128)(2,1)}, u32[]{:S(2)}) copy-start(bf16[512,2048]{1,0:T(8,128)(2,1)} %param.25) | copy-start | bytes 6291460
  6.5 39.9 %all-gather.11.cloned.1.call-start = ((), (), s32[]{:S(2)}) async-start(), calls=%async_computation.6 | async-start | bytes 1310720 | tf_op jit(solution)/shard_map/all_gather | solution.py:35
  15.0 32.1 %copy-start.5 = (f32[512]{0:T(512)S(1)}, f32[512]{0:T(512)}, u32[]{:S(2)}) copy-start(f32[512]{0:T(512)} %param.24) | copy-start | bytes 6148
  15.8 193.5 %reduce-scatter.3.cloned.1.call-start = ((), (), s32[]{:S(2)}) async-start(), calls=%async_computation.2 | async-start | bytes 655360 | tf_op jit(solution)/shard_map/reduce_scatter | solution.py:131
  28.8 17.7 %copy-start.2 = (f32[128,256]{1,0:T(8,128)S(1)}, f32[128,256]{1,0:T(8,128)}, u32[]{:S(2)}) copy-start(f32[128,256]{1,0:T(8,128)} %get-tuple-element.167) | copy-start | bytes 393220
  28.8 18.3 %copy-start.4 = (bf16[128,512]{1,0:T(8,128)(2,1)S(1)}, bf16[128,512]{1,0:T(8,128)(2,1)}, u32[]{:S(2)}) copy-start(bf16[128,512]{1,0:T(8,128)(2,1)} %param.21) | copy-start | bytes 393220
  48.6 193.5 %all-gather.7.cloned.1.call-start = ((), (), s32[]{:S(2)}) async-start(), calls=%async_computation.3 | async-start | bytes 7208960 | tf_op jit(solution)/shard_map/all_gather | solution.py:148
  49.3 300.3 %all-gather.9.cloned.1.call-start = ((), (), s32[]{:S(2)}) async-start(), calls=%async_computation.4 | async-start | bytes 7208960 | tf_op jit(solution)/shard_map/all_gather | solution.py:153
  49.9 326.9 %reduce-scatter.5.cloned.1.call-start = ((), (), s32[]{:S(2)}) async-start(), calls=%async_computation.5 | async-start | bytes 655360 | tf_op jit(solution)/shard_map/reduce_scatter | solution.py:160
  49.9 38.3 %collective-permute-start = (bf16[1408,512]{1,0:T(8,128)(2,1)}, bf16[1408,512]{1,0:T(8,128)(2,1)}, u32[]{:S(2)}, u32[]{:S(2)}) collective-permute-start(bf16[1408,512]{1,0:T(8,128)(2,1)} %param.29), channel_id=1, source_target_pairs={{0,4},{4,8},{8,12},{12,0},{1,5},{5,9},{9,13},{13,1},{2,6},{6,10},{... | collective-permute-start | bytes 4325384 | tf_op jit(solution)/shard_map/ppermute | solution.py:22
  52.8 153.9 %collective-permute-start.1 = (bf16[1408,512]{1,0:T(8,128)(2,1)}, bf16[1408,512]{1,0:T(8,128)(2,1)}, u32[]{:S(2)}, u32[]{:S(2)}) collective-permute-start(bf16[1408,512]{1,0:T(8,128)(2,1)} %param.29), channel_id=1, source_target_pairs={{0,12},{4,0},{8,4},{12,8},{1,13},{5,1},{9,5},{13,9},{2,14},{6,2},{... | collective-permute-start | bytes 4325384 | tf_op jit(solution)/shard_map/ppermute | solution.py:25
  58.7 150.6 %copy-start.3 = (bf16[128,2048]{1,0:T(8,128)(2,1)S(1)}, bf16[128,2048]{1,0:T(8,128)(2,1)}, u32[]{:S(2)}) copy-start(bf16[128,2048]{1,0:T(8,128)(2,1)} %param.17) | copy-start | bytes 1572868
  88.2 135.7 %collective-permute-start.2 = (bf16[1408,512]{1,0:T(8,128)(2,1)}, bf16[1408,512]{1,0:T(8,128)(2,1)}, u32[]{:S(2)}, u32[]{:S(2)}) collective-permute-start(bf16[1408,512]{1,0:T(8,128)(2,1)} %collective-permute-done), channel_id=1, source_target_pairs={{0,4},{4,8},{8,12},{12,0},{1,5},{5,9},{9,13},{13,1},{2,6},{6,10},{... | collective-permute-start | bytes 4325384 | tf_op jit(solution)/shard_map/ppermute | solution.py:22
  245.7 131.1 %copy-start.1 = (bf16[128,512]{1,0:T(8,128)(2,1)S(1)}, bf16[128,512]{1,0:T(8,128)(2,1)}, u32[]{:S(2)}) copy-start(bf16[128,512]{1,0:T(8,128)(2,1)} %reduce-scatter.3.cloned.1.call-done) | copy-start | bytes 393220
Sparse Core Ops, SparseCore 0:
  15.9 30.5 all-gather.10
  48.9 24.3 reduce-scatter.2
  74.9 167.0 all-gather.6
  243.5 106.0 all-gather.8
  356.8 19.8 reduce-scatter.4
